TPU v7x, 32 devices: a whole 2x2x4 slice. The times are simulated.
32 devices in a mesh: grp: 2 (over x), tp: 4 (over z), dp: 4 (over y, core).
Axes of the slice: x: 2, y: 2, z: 4, core: 2. Of those that a mesh axis runs over, the one named last changes fastest.
Arguments:
- hidden: bfloat16 [16, 2048], P('grp', 'dp'), parts along dimension 0, may hold values from -20 to 20
- lengths: int32 [16], P(('grp', 'dp')), parts along dimension 0, may hold values from 1 to 256, 512 in all
- input_norm_gain: float32 [2, 2048], P(None, 'dp'), may hold values from 0.1 to 1.9
- gate_matrix: bfloat16 [2, 2048, 4096], P(None, 'dp', 'tp'), may hold values from -0.125 to 0.125
- input_matrix: bfloat16 [2, 2048, 4096], P(None, 'dp', 'tp'), may hold values from -0.125 to 0.125
- write_matrix: bfloat16 [2, 2048, 2048], P(None, 'dp', 'tp'), may hold values from -0.125 to 0.125
- read_matrix: bfloat16 [2, 2048, 2048], P(None, 'dp', 'tp'), may hold values from -0.125 to 0.125
- step_matrix: bfloat16 [2, 2048, 64], P(None, 'dp'), may hold values from -0.125 to 0.125
- step_size_bias: float32 [2, 64], P(None, 'tp'), may hold values from -2 to 1
- log_decay_rate: float32 [2, 64], P(None, 'tp'), may hold values from -1 to 2
- direct_path_gain: float32 [2, 64], P(None, 'tp'), may hold values from 0.5 to 1.5
- input_filter_taps: bfloat16 [2, 4, 4096], P(None, None, 'tp'), may hold values from -3 to 3
- write_filter_taps: bfloat16 [2, 4, 2048], P(None, None, 'tp'), may hold values from -3 to 3
- read_filter_taps: bfloat16 [2, 4, 2048], P(None, None, 'tp'), may hold values from -3 to 3
- position_log_decay: float32 [2, 256, 64], P(None, None, 'tp'), may hold values from -0.7 to 0
- grouped_norm_gain: float32 [2, 4096], P(None, 'tp'), may hold values from 0.1 to 1.9
- output_matrix: bfloat16 [2, 4096, 2048], P(None, 'tp', 'dp'), may hold values from -0.09375 to 0.09375
- recurrent_head_state: float32 [2, 16, 64, 64, 128], P(None, ('grp', 'dp'), 'tp'), parts along dimension 1, may hold values from -3 to 3
- history_input_rows: bfloat16 [2, 16, 3, 4096], P(None, ('grp', 'dp'), None, 'tp'), parts along dimension 1, may hold values from -5 to 5
- history_write_rows: bfloat16 [2, 16, 3, 2048], P(None, ('grp', 'dp'), None, 'tp'), parts along dimension 1, may hold values from -5 to 5
- history_read_rows: bfloat16 [2, 16, 3, 2048], P(None, ('grp', 'dp'), None, 'tp'), parts along dimension 1, may hold values from -5 to 5
Outputs:
- stream_out: bfloat16 [16, 2048], P('grp', 'dp'), parts along dimension 0
- state_out: float32 [2, 16, 64, 64, 128], P(None, ('grp', 'dp'), 'tp'), parts along dimension 1
- buffer_value_out: bfloat16 [2, 16, 3, 4096], P(None, ('grp', 'dp'), None, 'tp'), parts along dimension 1
- buffer_write_out: bfloat16 [2, 16, 3, 2048], P(None, ('grp', 'dp'), None, 'tp'), parts along dimension 1
- buffer_read_out: bfloat16 [2, 16, 3, 2048], P(None, ('grp', 'dp'), None, 'tp'), parts along dimension 1
There are 2 independent parts, one for each index of `grp`. A program takes and returns all parts, laid end to end along the dimension named above; an argument that names none is the same for every part. Nothing has to cross between parts.
Inputs may be any that keep to these rules, and one draw needn't show every extreme that they name: `lengths`: a sequence's current token stands at position length - 1; some sequence has length 256.
All inputs are finite; a program needn't handle non-finite values. No bound on the sum of `lengths` on one device may be relied on, other than what follows from the above.
Results may differ from a plain program's by a relative error of at most 0.0065.
Values may be sent and summed in bfloat16 or wider, within the bound.
No kernel may reach another device: no remote copies, remote signals or barrier semaphores. Data moves between devices by JAX's collectives and lax.ppermute only.
A program may use at most 64 MiB of HBM per device.

v0:
```python
import jax
import jax.numpy as jnp
from jax import lax
from jax.sharding import PartitionSpec as P

D = 2048
epsilon = 1e-06


def convolve(buffer, new_row, weights, tap_valid):
    tap_rows = weights.astype(jnp.float32)
    depth = weights.shape[0] - 1
    summed = new_row.astype(jnp.float32) * tap_rows[depth]
    for k in range(depth):
        summed = summed + buffer[:, k].astype(jnp.float32) * tap_rows[k] * tap_valid[:, k : k + 1]
    shifted = jnp.concatenate([buffer[:, 1:], new_row[:, None]], axis=1)
    return (jax.nn.silu(summed), shifted)


def spread_groups(rows, seq_local, groups_local, per_group, state_dim):
    grouped = rows.reshape(seq_local, groups_local, 1, state_dim)
    return jnp.broadcast_to(grouped, (seq_local, groups_local, per_group, state_dim)).reshape(
        seq_local, groups_local * per_group, state_dim
    )


def on_device(
    hidden,
    lengths,
    input_norm_gain,
    gate_matrix,
    input_matrix,
    write_matrix,
    read_matrix,
    step_matrix,
    step_size_bias,
    log_decay_rate,
    direct_path_gain,
    input_filter_taps,
    write_filter_taps,
    read_filter_taps,
    position_log_decay,
    grouped_norm_gain,
    output_matrix,
    recurrent_head_state,
    history_input_rows,
    history_write_rows,
    history_read_rows,
):
    seq_local = lengths.shape[0]
    heads_local = step_size_bias.shape[1]
    head_dim = recurrent_head_state.shape[3]
    state_dim = recurrent_head_state.shape[4]
    groups_local = write_filter_taps.shape[2] // state_dim
    per_group = heads_local // groups_local
    inner_local = heads_local * head_dim
    shared_local = groups_local * state_dim
    depth = input_filter_taps.shape[1] - 1
    token_position = lengths - 1
    tap_valid = (jnp.arange(depth)[None, :] >= depth - token_position[:, None]).astype(jnp.float32)
    state_is_valid = (token_position > 0).astype(jnp.float32)[:, None]
    position_indicator = (
        token_position[:, None] == jnp.arange(position_log_decay.shape[1])[None, :]
    ).astype(jnp.float32)
    head_first = lax.axis_index("tp") * heads_local
    seq_first = lax.axis_index("dp") * seq_local
    share_rows = hidden.shape[0] // lax.axis_size("tp")
    share_first = lax.axis_index("tp") * share_rows
    stream = hidden
    states, values, writes, reads = ([], [], [], [])
    for layer_index in range(input_norm_gain.shape[0]):
        stream_float = stream.astype(jnp.float32)
        squares = jnp.sum(stream_float * stream_float, axis=1)
        normed = (stream_float * input_norm_gain[layer_index]).astype(jnp.bfloat16)
        pieces = [
            jnp.dot(normed, weight[layer_index], preferred_element_type=jnp.float32)
            for weight in (gate_matrix, input_matrix, write_matrix, read_matrix)
        ]
        joined = jnp.concatenate(pieces, axis=1)
        step_weight = step_matrix[layer_index]
        step_term = jnp.dot(normed, step_weight, preferred_element_type=jnp.float32)
        squares_all = lax.psum(squares, "dp")
        joined_mine, step_mine = (
            lax.psum_scatter(joined, "dp", scatter_dimension=0, tiled=True),
            lax.psum_scatter(step_term, "dp", scatter_dimension=0, tiled=True),
        )
        mean_square = lax.dynamic_slice_in_dim(squares_all, seq_first, seq_local, 0) / D
        row_scale = lax.rsqrt(mean_square + epsilon)[:, None]
        step_raw = lax.dynamic_slice_in_dim(step_mine, head_first, heads_local, 1) * row_scale
        scaled = joined_mine * row_scale
        proj_gate = scaled[:, :inner_local]
        value_row = scaled[:, inner_local : 2 * inner_local].astype(jnp.bfloat16)
        write_row = scaled[:, 2 * inner_local : 2 * inner_local + shared_local].astype(jnp.bfloat16)
        read_row = scaled[:, 2 * inner_local + shared_local :].astype(jnp.bfloat16)
        value_act, value_buf = convolve(
            history_input_rows[layer_index], value_row, input_filter_taps[layer_index], tap_valid
        )
        write_act, write_buf = convolve(
            history_write_rows[layer_index], write_row, write_filter_taps[layer_index], tap_valid
        )
        read_act, read_buf = convolve(
            history_read_rows[layer_index], read_row, read_filter_taps[layer_index], tap_valid
        )
        head_step_size = jax.nn.softplus(step_raw + step_size_bias[layer_index])
        current_log_decay = jnp.dot(
            position_indicator, position_log_decay[layer_index], precision=lax.Precision.HIGHEST
        )
        current_decay = (
            jnp.exp(-jnp.exp(log_decay_rate[layer_index]) * head_step_size + current_log_decay)
            * state_is_valid
        )
        value_heads = value_act.reshape(seq_local, heads_local, head_dim)
        write_heads = spread_groups(write_act, seq_local, groups_local, per_group, state_dim)
        read_heads = spread_groups(read_act, seq_local, groups_local, per_group, state_dim)
        updated = (
            current_decay[:, :, None, None] * recurrent_head_state[layer_index]
            + (head_step_size[:, :, None] * value_heads)[:, :, :, None] * write_heads[:, :, None, :]
        )
        readout = jnp.einsum("shpn,shn->shp", updated, read_heads, precision=lax.Precision.HIGHEST)
        mixed_heads = (
            readout + direct_path_gain[layer_index][None, :, None] * value_heads
        ) * jax.nn.silu(proj_gate.reshape(seq_local, heads_local, head_dim))
        grouped = mixed_heads.reshape(seq_local, groups_local, per_group * head_dim)
        grouped = grouped * lax.rsqrt(jnp.mean(grouped * grouped, axis=2, keepdims=True) + epsilon)
        gated_rows = (
            grouped.reshape(seq_local, inner_local) * grouped_norm_gain[layer_index]
        ).astype(jnp.bfloat16)
        out_weight = output_matrix[layer_index]

        def project(rows_in, first_row, out_weight=out_weight):
            return jnp.dot(rows_in, out_weight, preferred_element_type=jnp.float32)

        partial_out = project(lax.all_gather(gated_rows, "dp", axis=0, tiled=True), jnp.int32(0))
        branch_share = lax.psum_scatter(partial_out, "tp", scatter_dimension=0, tiled=True)
        stream_share = lax.dynamic_slice_in_dim(stream_float, share_first, share_rows, 0)
        new_share = (stream_share + branch_share).astype(jnp.bfloat16)
        stream = lax.all_gather(new_share, "tp", axis=0, tiled=True)
        states.append(updated)
        values.append(value_buf)
        writes.append(write_buf)
        reads.append(read_buf)
    return (stream, jnp.stack(states), jnp.stack(values), jnp.stack(writes), jnp.stack(reads))


def solution(mesh):
    placed = (
        P("grp", "dp"),
        P(("grp", "dp")),
        P(None, "dp"),
        P(None, "dp", "tp"),
        P(None, "dp", "tp"),
        P(None, "dp", "tp"),
        P(None, "dp", "tp"),
        P(None, "dp", None),
        P(None, "tp"),
        P(None, "tp"),
        P(None, "tp"),
        P(None, None, "tp"),
        P(None, None, "tp"),
        P(None, None, "tp"),
        P(None, None, "tp"),
        P(None, "tp"),
        P(None, "tp", "dp"),
        P(None, ("grp", "dp"), "tp", None, None),
        P(None, ("grp", "dp"), None, "tp"),
        P(None, ("grp", "dp"), None, "tp"),
        P(None, ("grp", "dp"), None, "tp"),
    )
    return jax.shard_map(
        on_device,
        mesh=mesh,
        in_specs=placed,
        out_specs=(
            P("grp", "dp"),
            P(None, ("grp", "dp"), "tp", None, None),
            P(None, ("grp", "dp"), None, "tp"),
            P(None, ("grp", "dp"), None, "tp"),
            P(None, ("grp", "dp"), None, "tp"),
        ),
        check_vma=False,
    )
```

profile of v0, /device:TPU:0, one launch (start us, length us, event | category | flops | bytes accessed | tf_op | source)
XLA Modules:
  0.0 185.2 jit_solution(15273092470525130623)
XLA Ops:
  7.4 0.8 fusion.114
  8.2 1.3 fusion.38
  9.5 1.2 fusion.36
  10.8 1.5 fusion.17
  12.5 0.7 pad_maximum_fusion.1
  16.1 8.5 %all-reduce.7 = (f32[8]{0:T(128)S(1)}, f32[8,64]{1,0:T(8,128)S(1)}) all-reduce(f32[8]{0:T(128)S(1)} %multiply_reduce_fusion.3, f32[8,64]{1,0:T(8,128)S(1)} %fusion.52), channel_id=1, replica_groups=mesh['grp'=2,'tp'=4,'dp'=4] {'dp'}, use_global_device_ids=true, to_apply=%region_2.0 | all-reduce | flops 520 | bytes 4160 | tf_op jit(solution)/shard_map/psum | solution.py:82
  25.5 1.5 fusion.2
  28.8 19.0 %all-reduce.11.cloned.1.call-done = f32[8,3072]{1,0:T(8,128)} async-done(((f32[8,3072]{1,0:T(8,128)}), f32[8,3072]{1,0:T(8,128)}) %all-reduce.11.cloned.1.call-update) | async-done | bytes 98320
  47.8 1.0 fusion.106
  48.8 0.8 divide_multiply_fusion.5
  49.9 0.8 broadcast_multiply_fusion.1
  50.7 3.1 %fusion.20 = f32[2,16,1,64]{3,2,1,0:T(1,128)S(1)} fusion(f32[2,16,128,1]{2,3,1,0:T(1,128)S(1)} %bitcast.277, f32[2,2,16,64,128]{4,3,2,1,0:T(8,128)} %param.38, f32[2,16,128]{2,1,0:T(8,128)S(1)} %bitcast.270, f32[2,16,64]{2,1,0:T(8,128)S(1)} %broadcast_multiply_fusion.1, f32[2,16]{1,0:T(2,128)} %fusion.2), kind=kOutput, calls=%fused_computation.24 | convolution fusion | flops 3932160 | bytes 1098752 | tf_op jit(solution)/shard_map/shpn,shn->shp/dot_general | solution.py:119
  53.8 0.8 multiply_reduce_fusion.2
  55.0 5.2 %all-gather = bf16[4,2,1024]{2,1,0:T(2,128)(2,1)S(1)} all-gather(bf16[1,2,1024]{2,1,0:T(2,128)(2,1)S(1)} %fusion.72), channel_id=1, replica_groups=mesh['grp'=2,'tp'=4,'dp'=4] {'dp'}, dimensions={0}, use_global_device_ids=true | all-gather | bytes 20480 | tf_op jit(solution)/shard_map/all_gather | solution.py:133
  60.2 1.5 fusion.13
  61.7 18.7 %all-reduce.2 = f32[8,512]{1,0:T(8,128)S(1)} all-reduce(f32[8,512]{1,0:T(8,128)S(1)} %fusion.13), channel_id=4, replica_groups=mesh['grp'=2,'tp'=4,'dp'=4] {'tp'}, use_global_device_ids=true, to_apply=%region_6.7.clone | all-reduce | flops 4096 | bytes 32768
  80.4 11.9 %all-gather.1 = bf16[4,2,512]{2,1,0:T(2,128)(2,1)S(1)} all-gather(bf16[1,2,512]{2,1,0:T(2,128)(2,1)S(1)} %fusion.100), channel_id=1, replica_groups=mesh['grp'=2,'tp'=4,'dp'=4] {'tp'}, dimensions={0}, use_global_device_ids=true | all-gather | bytes 10240 | tf_op jit(solution)/shard_map/all_gather | solution.py:137
  92.8 1.4 fusion.34
  94.7 5.9 %all-reduce.6 = (f32[8]{0:T(128)S(1)}, f32[8,64]{1,0:T(8,128)S(1)}) all-reduce(f32[8]{0:T(128)S(1)} %get-tuple-element.28, f32[8,64]{1,0:T(8,128)S(1)} %fusion.50), channel_id=1, replica_groups=mesh['grp'=2,'tp'=4,'dp'=4] {'dp'}, use_global_device_ids=true, to_apply=%region_9.10 | all-reduce | flops 520 | bytes 4160 | tf_op jit(solution)/shard_map/psum | solution.py:82
  100.8 0.7 pad_maximum_fusion.2
  101.6 0.9 fusion.3
  102.5 28.3 %all-reduce.13.cloned.1.call-done = f32[8,3072]{1,0:T(8,128)} async-done(((f32[8,3072]{1,0:T(8,128)}), f32[8,3072]{1,0:T(8,128)}) %all-reduce.13.cloned.1.call-update) | async-done | bytes 98320
  130.9 1.0 fusion.105
  132.4 2.2 %multiply_add_fusion.1 = (f32[1,2,16,64,128]{4,3,2,1,0:T(8,128)S(1)}, f32[1,2,16,64,128]{4,3,2,1,0:T(8,128)S(1)}) fusion(f32[2,2,16,64,128]{4,3,2,1,0:T(8,128)} %param.38, f32[2,16,128]{2,1,0:T(8,128)S(1)} %bitcast.271, f32[2,16,64]{2,1,0:T(8,128)S(1)} %broadcast_multiply_fusion.1, f32[2,16]{1,0:T(2,128)S(1)} %copy-done.19, f32[2,16,128]{2,1,0:T(8,128)S(1)} %bitcast.272, ...), kind=kLoop, calls=%fused_computation.26 | loop fusion | flops 1572864 | bytes 4243712 | tf_op jit(solution)/shard_map/add | solution.py:116
  134.6 1.9 %fusion.11 = f32[2,16,1,64]{3,2,1,0:T(1,128)S(1)} fusion(f32[2,16,128,1]{2,3,1,0:T(1,128)S(1)} %bitcast.276, f32[2,2,16,64,128]{4,3,2,1,0:T(8,128)S(1)} %copy-done.2, f32[2,16,128]{2,1,0:T(8,128)S(1)} %bitcast.273, f32[2,16,64]{2,1,0:T(8,128)S(1)} %broadcast_multiply_fusion, f32[2,16]{1,0:T(2,128)S(1)} %fusion.3), kind=kOutput, calls=%fused_computation.15 | convolution fusion | flops 3932160 | bytes 1106944 | tf_op jit(solution)/shard_map/shpn,shn->shp/dot_general | solution.py:119
  137.0 5.2 %all-gather.2 = bf16[4,2,1024]{2,1,0:T(2,128)(2,1)S(1)} all-gather(bf16[1,2,1024]{2,1,0:T(2,128)(2,1)S(1)} %fusion.73), channel_id=1, replica_groups=mesh['grp'=2,'tp'=4,'dp'=4] {'dp'}, dimensions={0}, use_global_device_ids=true | all-gather | bytes 20480 | tf_op jit(solution)/shard_map/all_gather | solution.py:133
  142.2 1.5 fusion.4
  143.7 18.7 %all-reduce.5 = f32[8,512]{1,0:T(8,128)S(1)} all-reduce(f32[8,512]{1,0:T(8,128)S(1)} %fusion.4), channel_id=7, replica_groups=mesh['grp'=2,'tp'=4,'dp'=4] {'tp'}, use_global_device_ids=true, to_apply=%region_13.14.clone | all-reduce | flops 4096 | bytes 32768
  162.4 11.9 %all-gather.3 = bf16[4,2,512]{2,1,0:T(2,128)(2,1)S(1)} all-gather(bf16[1,2,512]{2,1,0:T(2,128)(2,1)S(1)} %fusion.101), channel_id=1, replica_groups=mesh['grp'=2,'tp'=4,'dp'=4] {'tp'}, dimensions={0}, use_global_device_ids=true | all-gather | bytes 10240 | tf_op jit(solution)/shard_map/all_gather | solution.py:137
  175.6 0.6 pad_maximum_fusion.3
  176.3 0.6 pad_maximum_fusion.4
  176.9 1.5 pad_maximum_fusion
  (147 shorter events, 8.7 us)
Async XLA Ops:
  7.2 6.3 %copy-start.25 = (u32[32]{0:T(128)S(1)}, u32[32]{0:T(128)}, u32[]{:S(2)}) copy-start(u32[32]{0:T(128)} %constant.58) | copy-start | bytes 388
  7.2 5.1 %copy-start.4 = (bf16[8,512]{1,0:T(8,128)(2,1)S(1)}, bf16[8,512]{1,0:T(8,128)(2,1)}, u32[]{:S(2)}) copy-start(bf16[8,512]{1,0:T(8,128)(2,1)} %param.21) | copy-start | bytes 24580
  7.2 5.1 %copy-start = (bf16[2,512,1024]{2,1,0:T(8,128)(2,1)S(1)}, bf16[2,512,1024]{2,1,0:T(8,128)(2,1)}, u32[]{:S(2)}) copy-start(bf16[2,512,1024]{2,1,0:T(8,128)(2,1)} %param.25) | copy-start | bytes 6291460
  7.2 6.2 %copy-start.21 = (s32[2]{0:T(128)S(1)}, s32[2]{0:T(128)}, u32[]{:S(2)}) copy-start(s32[2]{0:T(128)} %param.22) | copy-start | bytes 28
  7.2 7.5 %copy-start.16 = (f32[2,16]{1,0:T(2,128)S(1)}, f32[2,16]{1,0:T(2,128)}, u32[]{:S(2)}) copy-start(f32[2,16]{1,0:T(2,128)} %param.29) | copy-start | bytes 388
  7.2 8.0 %copy-start.17 = (f32[2,16]{1,0:T(2,128)S(1)}, f32[2,16]{1,0:T(2,128)}, u32[]{:S(2)}) copy-start(f32[2,16]{1,0:T(2,128)} %param.30) | copy-start | bytes 388
  7.2 8.6 %copy-start.5 = (bf16[2,512,64]{1,2,0:T(8,128)(2,1)S(1)}, bf16[2,512,64]{1,2,0:T(8,128)(2,1)}, u32[]{:S(2)}) copy-start(bf16[2,512,64]{1,2,0:T(8,128)(2,1)} %param.28) | copy-start | bytes 393220
  7.2 8.7 %copy-start.12 = (f32[2,1024]{1,0:T(2,128)S(1)}, f32[2,1024]{1,0:T(2,128)}, u32[]{:S(2)}) copy-start(f32[2,1024]{1,0:T(2,128)} %param.36) | copy-start | bytes 24580
  7.3 8.7 %copy-start.10 = (bf16[2,4,512]{2,1,0:T(4,128)(2,1)S(1)}, bf16[2,4,512]{2,1,0:T(4,128)(2,1)}, u32[]{:S(2)}) copy-start(bf16[2,4,512]{2,1,0:T(4,128)(2,1)} %param.33) | copy-start | bytes 24580
  7.3 8.7 %copy-start.11 = (bf16[2,4,512]{2,1,0:T(4,128)(2,1)S(1)}, bf16[2,4,512]{2,1,0:T(4,128)(2,1)}, u32[]{:S(2)}) copy-start(bf16[2,4,512]{2,1,0:T(4,128)(2,1)} %param.34) | copy-start | bytes 24580
  7.3 8.7 %copy-start.6 = (bf16[2,2,3,1024]{3,1,2,0:T(2,128)(2,1)S(1)}, bf16[2,2,3,1024]{3,1,2,0:T(2,128)(2,1)}, u32[]{:S(2)}) copy-start(bf16[2,2,3,1024]{3,1,2,0:T(2,128)(2,1)} %param.39) | copy-start | bytes 73732
  7.3 8.7 %copy-start.7 = (bf16[2,4,1024]{2,1,0:T(4,128)(2,1)S(1)}, bf16[2,4,1024]{2,1,0:T(4,128)(2,1)}, u32[]{:S(2)}) copy-start(bf16[2,4,1024]{2,1,0:T(4,128)(2,1)} %param.32) | copy-start | bytes 49156
  7.3 18.0 %copy-start.8 = (bf16[2,2,3,512]{3,1,2,0:T(2,128)(2,1)S(1)}, bf16[2,2,3,512]{3,1,2,0:T(2,128)(2,1)}, u32[]{:S(2)}) copy-start(bf16[2,2,3,512]{3,1,2,0:T(2,128)(2,1)} %param.41) | copy-start | bytes 36868
  7.3 18.0 %copy-start.9 = (bf16[2,2,3,512]{3,1,2,0:T(2,128)(2,1)S(1)}, bf16[2,2,3,512]{3,1,2,0:T(2,128)(2,1)}, u32[]{:S(2)}) copy-start(bf16[2,2,3,512]{3,1,2,0:T(2,128)(2,1)} %param.40) | copy-start | bytes 36868
  7.3 40.5 %all-reduce.11.cloned.1.call-start = ((), (), s32[]{:S(2)}) async-start(), calls=%async_computation | async-start | bytes 196608
  8.2 18.8 %copy-start.18 = (f32[2,16]{1,0:T(2,128)S(1)}, f32[2,16]{1,0:T(2,128)}, u32[]{:S(2)}) copy-start(f32[2,16]{1,0:T(2,128)} %param.31) | copy-start | bytes 388
  8.2 19.4 %copy-start.24 = (u32[32]{0:T(128)S(1)}, u32[32]{0:T(128)}, u32[]{:S(2)}) copy-start(u32[32]{0:T(128)} %constant.66) | copy-start | bytes 388
  12.5 80.1 %copy-start.3 = (bf16[2,512,512]{2,1,0:T(8,128)(2,1)S(1)}, bf16[2,512,512]{2,1,0:T(8,128)(2,1)}, u32[]{:S(2)}) copy-start(bf16[2,512,512]{2,1,0:T(8,128)(2,1)} %param.27) | copy-start | bytes 3145732
  13.2 117.7 %all-reduce.13.cloned.1.call-start = ((), (), s32[]{:S(2)}) async-start(), calls=%async_computation.1 | async-start | bytes 196608
  13.4 14.2 %copy-start.26 = (f32[2]{0:T(128)}, f32[2]{0:T(128)S(1)}, u32[]{:S(2)}) copy-start(f32[2]{0:T(128)S(1)} %compare_convert_fusion) | copy-start | bytes 28
  13.4 14.2 %copy-start.22 = (s32[2]{0:T(128)}, s32[2]{0:T(128)S(1)}, u32[]{:S(2)}) copy-start(s32[2]{0:T(128)S(1)} %get-tuple-element.78) | copy-start | bytes 28
  25.5 3.4 %copy-start.13 = (f32[2,16]{1,0:T(2,128)}, f32[2,16]{1,0:T(2,128)S(1)}, u32[]{:S(2)}) copy-start(f32[2,16]{1,0:T(2,128)S(1)} %compare_select_fusion.1) | copy-start | bytes 388
  61.7 39.8 %copy-start.15 = (f32[16]{0:T(128)S(1)}, f32[16]{0:T(128)}, u32[]{:S(2)}) copy-start(f32[16]{0:T(128)} %get-tuple-element.76) | copy-start | bytes 196
  61.7 39.9 %copy-start.20 = (f32[16]{0:T(128)S(1)}, f32[16]{0:T(128)}, u32[]{:S(2)}) copy-start(f32[16]{0:T(128)} %get-tuple-element.74) | copy-start | bytes 196
  61.7 39.9 %copy-start.23 = (s32[2]{0:T(128)S(1)}, s32[2]{0:T(128)}, u32[]{:S(2)}) copy-start(s32[2]{0:T(128)} %copy-done.22) | copy-start | bytes 28
  61.7 39.9 %copy-start.27 = (f32[2]{0:T(128)S(1)}, f32[2]{0:T(128)}, u32[]{:S(2)}) copy-start(f32[2]{0:T(128)} %copy-done.26) | copy-start | bytes 28
  92.4 2.1 %copy-start.1 = (bf16[2,512,1024]{2,1,0:T(8,128)(2,1)S(1)}, bf16[2,512,1024]{2,1,0:T(8,128)(2,1)}, u32[]{:S(2)}) copy-start(bf16[2,512,1024]{2,1,0:T(8,128)(2,1)} %param.24) | copy-start | bytes 6291460
  92.5 39.9 %copy-start.19 = (f32[2,16]{1,0:T(2,128)S(1)}, f32[2,16]{1,0:T(2,128)}, u32[]{:S(2)}) copy-start(f32[2,16]{1,0:T(2,128)} %fusion.2) | copy-start | bytes 388
  132.4 2.2 %copy-start.2 = (f32[2,2,16,64,128]{4,3,2,1,0:T(8,128)S(1)}, f32[2,2,16,64,128]{4,3,2,1,0:T(8,128)}, u32[]{:S(2)}) copy-start(f32[2,2,16,64,128]{4,3,2,1,0:T(8,128)} %param.38) | copy-start | bytes 6291460
  132.4 4.1 %copy-start.14 = (f32[16]{0:T(128)S(1)}, f32[16]{0:T(128)}, u32[]{:S(2)}) copy-start(f32[16]{0:T(128)} %get-tuple-element.72) | copy-start | bytes 196
Sparse Core Ops, SparseCore 0:
  13.3 34.4 all-reduce.10
  101.6 29.2 all-reduce.12
where the time goes:
time: 186 us; the launch traced here: 185 us
  blocking collectives  86.2 us (46%)
  waiting for transfers between devices  47.3 us (25%)
  matrix products  16.9 us (9%)
  between operations  15.9 us (9%)
  other arithmetic  13.2 us (7%)
  local copies, waits for them, and re-layouts  5.54 us (3%)
    unnamed x4, waiting for transfers between devices  47.3 us
    unnamed x2, blocking collectives  37.4 us
    all_gather x2, blocking collectives, on_device(): stream = lax.all_gather(new_share, 'tp', axis=0, tiled=True)  23.9 us
    psum x2, blocking collectives, on_device(): squares_all = lax.psum(squares, 'dp')  14.5 us
    all_gather x2, blocking collectives, on_device(): lax.all_gather(gated_rows, 'dp', axis=0, tiled=True)  10.4 us
    dot_general x8, matrix products, on_device(): jnp.dot(normed, weight[layer_index], preferred_element_type=jnp.float32)  6.41 us
    dot_general x2, matrix products, on_device(): jnp.einsum('shpn,shn->shp', updated, read_heads, precision=lax.Precision....  4.94 us
  transfers between devices with their start and end apart: 2, of which 2 were waited for; matrix products, arithmetic and copies ran while one was open for 4% of the time, Pallas kernels for 0%

commit v1 on v0

--- a/solution.py
+++ b/solution.py
@@ -134,7 +134,10 @@
         branch_share = lax.psum_scatter(partial_out, "tp", scatter_dimension=0, tiled=True)
         stream_share = lax.dynamic_slice_in_dim(stream_float, share_first, share_rows, 0)
         new_share = (stream_share + branch_share).astype(jnp.bfloat16)
-        stream = lax.all_gather(new_share, "tp", axis=0, tiled=True)
+        devices = lax.axis_size("tp")
+        parts = jnp.stack([new_share for _ in range(devices)])
+        parts = lax.all_to_all(parts, "tp", split_axis=0, concat_axis=0)
+        stream = jnp.concatenate(parts, axis=0)
         states.append(updated)
         values.append(value_buf)
         writes.append(write_buf)

time: 186 us -> 176 us (0.946)
  blocking collectives: 86.2 us -> 62.6 us
  waiting for transfers between devices: 47.3 us -> 54.7 us
  starting transfers between devices: 0.08 us -> 6.58 us
    all_gather x2 -> x0, blocking collectives: 23.9 us -> none  [on_device(): stream = lax.all_gather(new_share, 'tp', axis=0, tiled=True)]
    all_to_all x0 -> x2, waiting for transfers between devices: none -> 7.52 us  [on_device(): parts = lax.all_to_all(parts, 'tp', split_axis=0, concat_axis=0)]
    all_to_all x0 -> x2, starting transfers between devices: none -> 6.5 us  [on_device(): parts = lax.all_to_all(parts, 'tp', split_axis=0, concat_axis=0)]
  transfers between devices with their start and end apart: 2 -> 4, of which waited for: 2 -> 4; matrix products, arithmetic and copies ran while one was open for 4% -> 6% of each run, Pallas kernels for 0% -> 0%
where the time goes in v1:
time: 176 us; the launch traced here: 175 us
  blocking collectives  62.6 us (36%)
  waiting for transfers between devices  54.7 us (31%)
  matrix products  16.2 us (9%)
  between operations  15.9 us (9%)
  other arithmetic  12.4 us (7%)
  local copies, waits for them, and re-layouts  6.89 us (4%)
  starting transfers between devices  6.58 us (4%)
    unnamed x4, waiting for transfers between devices  47.2 us
    unnamed x2, blocking collectives  37.6 us
    psum x2, blocking collectives, on_device(): squares_all = lax.psum(squares, 'dp')  14.6 us
    all_gather x2, blocking collectives, on_device(): lax.all_gather(gated_rows, 'dp', axis=0, tiled=True)  10.4 us
    all_to_all x2, waiting for transfers between devices, on_device(): parts = lax.all_to_all(parts, 'tp', split_axis=0, concat_axis=0)  7.52 us
    all_to_all x2, starting transfers between devices, on_device(): parts = lax.all_to_all(parts, 'tp', split_axis=0, concat_axis=0)  6.5 us
    dot_general x8, matrix products, on_device(): jnp.dot(normed, weight[layer_index], preferred_element_type=jnp.float32)  6.46 us
    dot_general x2, matrix products, on_device(): jnp.einsum('shpn,shn->shp', updated, read_heads, precision=lax.Precision....  4.93 us
  transfers between devices with their start and end apart: 4, of which 4 were waited for; matrix products, arithmetic and copies ran while one was open for 6% of the time, Pallas kernels for 0%

profile of v1, /device:TPU:0, one launch (start us, length us, event | category | flops | bytes accessed | tf_op | source)
XLA Modules:
  0.0 175.3 jit_solution(7389809470750810611)
XLA Ops:
  7.4 0.8 fusion.112
  8.2 1.3 fusion.38
  9.5 1.2 fusion.36
  10.8 1.5 fusion.17
  12.5 0.7 pad_maximum_fusion.1
  16.5 8.6 %all-reduce.7 = (f32[8]{0:T(128)S(1)}, f32[8,64]{1,0:T(8,128)S(1)}) all-reduce(f32[8]{0:T(128)S(1)} %multiply_reduce_fusion.3, f32[8,64]{1,0:T(8,128)S(1)} %fusion.52), channel_id=1, replica_groups=mesh['grp'=2,'tp'=4,'dp'=4] {'dp'}, use_global_device_ids=true, to_apply=%region_2.0 | all-reduce | flops 520 | bytes 4160 | tf_op jit(solution)/shard_map/psum | solution.py:82
  25.4 1.5 fusion.2
  27.4 1.3 dynamic-slice.4
  29.4 18.4 %all-reduce.11.cloned.1.call-done = f32[8,3072]{1,0:T(8,128)} async-done(((f32[8,3072]{1,0:T(8,128)}), f32[8,3072]{1,0:T(8,128)}) %all-reduce.11.cloned.1.call-update) | async-done | bytes 98320
  47.7 1.0 fusion.104
  49.2 3.1 %fusion.20 = f32[2,16,1,64]{3,2,1,0:T(1,128)S(1)} fusion(f32[2,16,128,1]{2,3,1,0:T(1,128)S(1)} %bitcast.273, f32[2,2,16,64,128]{4,3,2,1,0:T(8,128)} %param.38, f32[2,16,128]{2,1,0:T(8,128)S(1)} %bitcast.266, f32[2,16,64]{2,1,0:T(8,128)S(1)} %broadcast_multiply_fusion.1, f32[2,16]{1,0:T(2,128)} %fusion.2), kind=kOutput, calls=%fused_computation.24 | convolution fusion | flops 3932160 | bytes 1098752 | tf_op jit(solution)/shard_map/shpn,shn->shp/dot_general | solution.py:119
  52.3 0.8 multiply_reduce_fusion.2
  53.5 5.2 %all-gather = bf16[4,2,1024]{2,1,0:T(2,128)(2,1)S(1)} all-gather(bf16[1,2,1024]{2,1,0:T(2,128)(2,1)S(1)} %fusion.72), channel_id=1, replica_groups=mesh['grp'=2,'tp'=4,'dp'=4] {'dp'}, dimensions={0}, use_global_device_ids=true | all-gather | bytes 20480 | tf_op jit(solution)/shard_map/all_gather | solution.py:133
  58.7 1.5 fusion.13
  60.2 18.9 %all-reduce.2 = f32[8,512]{1,0:T(8,128)S(1)} all-reduce(f32[8,512]{1,0:T(8,128)S(1)} %fusion.13), channel_id=4, replica_groups=mesh['grp'=2,'tp'=4,'dp'=4] {'tp'}, use_global_device_ids=true, to_apply=%region_6.7.clone | all-reduce | flops 4096 | bytes 32768
  79.7 3.2 %all-to-all-start = ((bf16[4,2,512]{2,1,0:T(2,128)(2,1)}), bf16[4,2,512]{2,1,0:T(2,128)(2,1)S(1)}, u32[]{:S(2)}, u32[]{:S(2)}) async-start(bf16[4,2,512]{2,1,0:T(2,128)(2,1)} %stack.46), calls=%async_computation | async-start | bytes 16384 | tf_op jit(solution)/shard_map/all_to_all | solution.py:139
  83.1 5.4 %all-to-all-done = bf16[4,2,512]{2,1,0:T(2,128)(2,1)S(1)} async-done(((bf16[4,2,512]{2,1,0:T(2,128)(2,1)}), bf16[4,2,512]{2,1,0:T(2,128)(2,1)S(1)}, u32[]{:S(2)}, u32[]{:S(2)}) %all-to-all-start) | async-done | bytes 8224 | tf_op jit(solution)/shard_map/all_to_all | solution.py:139
  89.2 1.5 fusion.8
  91.0 6.0 %all-reduce.6 = (f32[8]{0:T(128)S(1)}, f32[8,64]{1,0:T(8,128)S(1)}) all-reduce(f32[8]{0:T(128)S(1)} %reduce_sum.57, f32[8,64]{1,0:T(8,128)S(1)} %fusion.50), channel_id=1, replica_groups=mesh['grp'=2,'tp'=4,'dp'=4] {'dp'}, use_global_device_ids=true, to_apply=%region_9.10 | all-reduce | flops 520 | bytes 4160 | tf_op jit(solution)/shard_map/psum | solution.py:82
  97.0 0.7 pad_maximum_fusion.2
  98.1 28.8 %all-reduce.13.cloned.1.call-done = f32[8,3072]{1,0:T(8,128)} async-done(((f32[8,3072]{1,0:T(8,128)}), f32[8,3072]{1,0:T(8,128)}) %all-reduce.13.cloned.1.call-update) | async-done | bytes 98320
  126.9 1.0 fusion.103
  128.4 2.2 %multiply_add_fusion.1 = (f32[1,2,16,64,128]{4,3,2,1,0:T(8,128)S(1)}, f32[1,2,16,64,128]{4,3,2,1,0:T(8,128)S(1)}) fusion(f32[2,2,16,64,128]{4,3,2,1,0:T(8,128)} %param.38, f32[2,16,128]{2,1,0:T(8,128)S(1)} %bitcast.267, f32[2,16,64]{2,1,0:T(8,128)S(1)} %broadcast_multiply_fusion.1, f32[2,16]{1,0:T(2,128)S(1)} %copy-done.17, f32[2,16,128]{2,1,0:T(8,128)S(1)} %bitcast.268, ...), kind=kLoop, calls=%fused_computation.26 | loop fusion | flops 1572864 | bytes 4243712 | tf_op jit(solution)/shard_map/add | solution.py:116
  130.6 1.9 %fusion.11 = f32[2,16,1,64]{3,2,1,0:T(1,128)S(1)} fusion(f32[2,16,128,1]{2,3,1,0:T(1,128)S(1)} %bitcast.272, f32[2,2,16,64,128]{4,3,2,1,0:T(8,128)S(1)} %copy-done.1, f32[2,16,128]{2,1,0:T(8,128)S(1)} %bitcast.269, f32[2,16,64]{2,1,0:T(8,128)S(1)} %broadcast_multiply_fusion, f32[2,16]{1,0:T(2,128)S(1)} %fusion.3), kind=kOutput, calls=%fused_computation.15 | convolution fusion | flops 3932160 | bytes 1106944 | tf_op jit(solution)/shard_map/shpn,shn->shp/dot_general | solution.py:119
  133.0 5.2 %all-gather.1 = bf16[4,2,1024]{2,1,0:T(2,128)(2,1)S(1)} all-gather(bf16[1,2,1024]{2,1,0:T(2,128)(2,1)S(1)} %fusion.73), channel_id=1, replica_groups=mesh['grp'=2,'tp'=4,'dp'=4] {'dp'}, dimensions={0}, use_global_device_ids=true | all-gather | bytes 20480 | tf_op jit(solution)/shard_map/all_gather | solution.py:133
  138.2 1.5 fusion.4
  139.7 18.7 %all-reduce.5 = f32[8,512]{1,0:T(8,128)S(1)} all-reduce(f32[8,512]{1,0:T(8,128)S(1)} %fusion.4), channel_id=7, replica_groups=mesh['grp'=2,'tp'=4,'dp'=4] {'tp'}, use_global_device_ids=true, to_apply=%region_13.14.clone | all-reduce | flops 4096 | bytes 32768
  159.0 3.2 %all-to-all-start.1 = ((bf16[4,2,512]{2,1,0:T(2,128)(2,1)}), bf16[4,2,512]{2,1,0:T(2,128)(2,1)S(1)}, u32[]{:S(2)}, u32[]{:S(2)}) async-start(bf16[4,2,512]{2,1,0:T(2,128)(2,1)} %stack.47), calls=%async_computation.1 | async-start | bytes 16384 | tf_op jit(solution)/shard_map/all_to_all | solution.py:139
  162.3 0.6 pad_maximum_fusion.5
  162.9 0.6 pad_maximum_fusion.3
  163.6 1.5 pad_maximum_fusion
  165.7 2.1 %all-to-all-done.1 = bf16[4,2,512]{2,1,0:T(2,128)(2,1)S(1)} async-done(((bf16[4,2,512]{2,1,0:T(2,128)(2,1)}), bf16[4,2,512]{2,1,0:T(2,128)(2,1)S(1)}, u32[]{:S(2)}, u32[]{:S(2)}) %all-to-all-start.1) | async-done | bytes 8224 | tf_op jit(solution)/shard_map/all_to_all | solution.py:139
  (147 shorter events, 9.5 us)
Async XLA Ops:
  7.2 6.7 %copy-start.23 = (u32[32]{0:T(128)S(1)}, u32[32]{0:T(128)}, u32[]{:S(2)}) copy-start(u32[32]{0:T(128)} %constant.58) | copy-start | bytes 388
  7.2 5.1 %copy-start.4 = (bf16[8,512]{1,0:T(8,128)(2,1)S(1)}, bf16[8,512]{1,0:T(8,128)(2,1)}, u32[]{:S(2)}) copy-start(bf16[8,512]{1,0:T(8,128)(2,1)} %param.21) | copy-start | bytes 24580
  7.2 5.1 %copy-start = (bf16[2,512,1024]{2,1,0:T(8,128)(2,1)S(1)}, bf16[2,512,1024]{2,1,0:T(8,128)(2,1)}, u32[]{:S(2)}) copy-start(bf16[2,512,1024]{2,1,0:T(8,128)(2,1)} %param.25) | copy-start | bytes 6291460
  7.2 6.1 %copy-start.20 = (s32[2]{0:T(128)S(1)}, s32[2]{0:T(128)}, u32[]{:S(2)}) copy-start(s32[2]{0:T(128)} %param.22) | copy-start | bytes 28
  7.2 7.9 %copy-start.14 = (f32[2,16]{1,0:T(2,128)S(1)}, f32[2,16]{1,0:T(2,128)}, u32[]{:S(2)}) copy-start(f32[2,16]{1,0:T(2,128)} %param.29) | copy-start | bytes 388
  7.2 8.4 %copy-start.15 = (f32[2,16]{1,0:T(2,128)S(1)}, f32[2,16]{1,0:T(2,128)}, u32[]{:S(2)}) copy-start(f32[2,16]{1,0:T(2,128)} %param.30) | copy-start | bytes 388
  7.2 9.0 %copy-start.5 = (bf16[2,512,64]{1,2,0:T(8,128)(2,1)S(1)}, bf16[2,512,64]{1,2,0:T(8,128)(2,1)}, u32[]{:S(2)}) copy-start(bf16[2,512,64]{1,2,0:T(8,128)(2,1)} %param.28) | copy-start | bytes 393220
  7.2 9.1 %copy-start.12 = (f32[2,1024]{1,0:T(2,128)S(1)}, f32[2,1024]{1,0:T(2,128)}, u32[]{:S(2)}) copy-start(f32[2,1024]{1,0:T(2,128)} %param.36) | copy-start | bytes 24580
  7.3 9.1 %copy-start.10 = (bf16[2,4,512]{2,1,0:T(4,128)(2,1)S(1)}, bf16[2,4,512]{2,1,0:T(4,128)(2,1)}, u32[]{:S(2)}) copy-start(bf16[2,4,512]{2,1,0:T(4,128)(2,1)} %param.33) | copy-start | bytes 24580
  7.3 9.1 %copy-start.11 = (bf16[2,4,512]{2,1,0:T(4,128)(2,1)S(1)}, bf16[2,4,512]{2,1,0:T(4,128)(2,1)}, u32[]{:S(2)}) copy-start(bf16[2,4,512]{2,1,0:T(4,128)(2,1)} %param.34) | copy-start | bytes 24580
  7.3 9.1 %copy-start.6 = (bf16[2,2,3,1024]{3,1,2,0:T(2,128)(2,1)S(1)}, bf16[2,2,3,1024]{3,1,2,0:T(2,128)(2,1)}, u32[]{:S(2)}) copy-start(bf16[2,2,3,1024]{3,1,2,0:T(2,128)(2,1)} %param.39) | copy-start | bytes 73732
  7.3 9.2 %copy-start.7 = (bf16[2,4,1024]{2,1,0:T(4,128)(2,1)S(1)}, bf16[2,4,1024]{2,1,0:T(4,128)(2,1)}, u32[]{:S(2)}) copy-start(bf16[2,4,1024]{2,1,0:T(4,128)(2,1)} %param.32) | copy-start | bytes 49156
  7.3 17.9 %copy-start.8 = (bf16[2,2,3,512]{3,1,2,0:T(2,128)(2,1)S(1)}, bf16[2,2,3,512]{3,1,2,0:T(2,128)(2,1)}, u32[]{:S(2)}) copy-start(bf16[2,2,3,512]{3,1,2,0:T(2,128)(2,1)} %param.41) | copy-start | bytes 36868
  7.3 17.9 %copy-start.9 = (bf16[2,2,3,512]{3,1,2,0:T(2,128)(2,1)S(1)}, bf16[2,2,3,512]{3,1,2,0:T(2,128)(2,1)}, u32[]{:S(2)}) copy-start(bf16[2,2,3,512]{3,1,2,0:T(2,128)(2,1)} %param.40) | copy-start | bytes 36868
  7.3 40.4 %all-reduce.11.cloned.1.call-start = ((), (), s32[]{:S(2)}) async-start(), calls=%async_computation.2 | async-start | bytes 196608
  8.2 18.7 %copy-start.16 = (f32[2,16]{1,0:T(2,128)S(1)}, f32[2,16]{1,0:T(2,128)}, u32[]{:S(2)}) copy-start(f32[2,16]{1,0:T(2,128)} %param.31) | copy-start | bytes 388
  13.2 75.6 %copy-start.2 = (bf16[2,512,512]{2,1,0:T(8,128)(2,1)S(1)}, bf16[2,512,512]{2,1,0:T(8,128)(2,1)}, u32[]{:S(2)}) copy-start(bf16[2,512,512]{2,1,0:T(8,128)(2,1)} %param.27) | copy-start | bytes 3145732
  13.8 11.6 %copy-start.21 = (s32[2]{0:T(128)}, s32[2]{0:T(128)S(1)}, u32[]{:S(2)}) copy-start(s32[2]{0:T(128)S(1)} %get-tuple-element.78) | copy-start | bytes 28
  60.2 37.5 %copy-start.13 = (f32[16]{0:T(128)S(1)}, f32[16]{0:T(128)}, u32[]{:S(2)}) copy-start(f32[16]{0:T(128)} %get-tuple-element.76) | copy-start | bytes 196
  60.2 37.6 %copy-start.18 = (f32[16]{0:T(128)S(1)}, f32[16]{0:T(128)}, u32[]{:S(2)}) copy-start(f32[16]{0:T(128)} %get-tuple-element.74) | copy-start | bytes 196
  60.2 37.6 %copy-start.19 = (f32[2,256,16]{1,2,0:T(8,128)S(1)}, f32[2,256,16]{1,2,0:T(8,128)}, u32[]{:S(2)}) copy-start(f32[2,256,16]{1,2,0:T(8,128)} %param.35) | copy-start | bytes 98308
  60.2 37.6 %copy-start.22 = (s32[2]{0:T(128)S(1)}, s32[2]{0:T(128)}, u32[]{:S(2)}) copy-start(s32[2]{0:T(128)} %copy-done.21) | copy-start | bytes 28
  79.1 18.8 %copy-start.24 = (f32[2]{0:T(128)S(1)}, f32[2]{0:T(128)}, u32[]{:S(2)}) copy-start(f32[2]{0:T(128)} %compare_convert_fusion) | copy-start | bytes 28
  79.7 8.8 %all-to-all-start = ((bf16[4,2,512]{2,1,0:T(2,128)(2,1)}), bf16[4,2,512]{2,1,0:T(2,128)(2,1)S(1)}, u32[]{:S(2)}, u32[]{:S(2)}) async-start(bf16[4,2,512]{2,1,0:T(2,128)(2,1)} %stack.46), calls=%async_computation | async-start | bytes 16384 | tf_op jit(solution)/shard_map/all_to_all | solution.py:139
  83.0 43.9 %all-reduce.13.cloned.1.call-start = ((), (), s32[]{:S(2)}) async-start(), calls=%async_computation.3 | async-start | bytes 196608
  88.6 39.7 %copy-start.17 = (f32[2,16]{1,0:T(2,128)S(1)}, f32[2,16]{1,0:T(2,128)}, u32[]{:S(2)}) copy-start(f32[2,16]{1,0:T(2,128)} %fusion.2) | copy-start | bytes 388
  88.9 1.9 %copy-start.3 = (bf16[2,512,512]{2,1,0:T(8,128)(2,1)S(1)}, bf16[2,512,512]{2,1,0:T(8,128)(2,1)}, u32[]{:S(2)}) copy-start(bf16[2,512,512]{2,1,0:T(8,128)(2,1)} %param.26) | copy-start | bytes 3145732
  128.4 2.2 %copy-start.1 = (f32[2,2,16,64,128]{4,3,2,1,0:T(8,128)S(1)}, f32[2,2,16,64,128]{4,3,2,1,0:T(8,128)}, u32[]{:S(2)}) copy-start(f32[2,2,16,64,128]{4,3,2,1,0:T(8,128)} %param.38) | copy-start | bytes 6291460
  159.0 8.8 %all-to-all-start.1 = ((bf16[4,2,512]{2,1,0:T(2,128)(2,1)}), bf16[4,2,512]{2,1,0:T(2,128)(2,1)S(1)}, u32[]{:S(2)}, u32[]{:S(2)}) async-start(bf16[4,2,512]{2,1,0:T(2,128)(2,1)} %stack.47), calls=%async_computation.1 | async-start | bytes 16384 | tf_op jit(solution)/shard_map/all_to_all | solution.py:139
Sparse Core Ops, SparseCore 0:
  13.3 34.3 all-reduce.10
  97.8 28.9 all-reduce.12
